TPU v7x, 32 devices: a whole 2x2x4 slice. The times are simulated.
32 devices in a mesh: sp: 8 (over z, x), tp: 4 (over y, core).
Axes of the slice: x: 2, y: 2, z: 4, core: 2. Of those that a mesh axis runs over, the one named last changes fastest.
Arguments:
- queries: bfloat16 [1024, 32, 128], P('sp', 'tp'), may hold values from -6 to 6
- keys: bfloat16 [1024, 8, 128], P('sp', 'tp'), may hold values from -6 to 6
- values: bfloat16 [1024, 8, 128], P('sp', 'tp'), may hold values from -6 to 6
- q_gain: float32 [128], replicated, may hold values from 0.2 to 8
- k_gain: float32 [128], replicated, may hold values from 0.2 to 8
- w_out: bfloat16 [4096, 2048], P('tp'), may hold values from -0.09375 to 0.09375
- residual: bfloat16 [1024, 2048], P(('sp', 'tp')), may hold values from -6 to 6
- gain_mix: float32 [2048], replicated, may hold values from 0.1 to 1.9
- gain_pre: float32 [2048], replicated, may hold values from 0.1 to 1.9
- routes: int32 [1024, 4], P(('sp', 'tp')), may hold values from 0 to 7, all different within a row; in each aligned block of 32 rows (0 to 31, 32 to 63, ...) at most 32 rows name the same one
- route_weights: float32 [1024, 4], P(('sp', 'tp')), may hold values from 0.1 to 1
- w_gate: bfloat16 [8, 2048, 2048], P('sp', None, 'tp'), may hold values from -0.5 to 0.5
- w_up: bfloat16 [8, 2048, 2048], P('sp', None, 'tp'), may hold values from -0.5 to 0.5
- w_down: bfloat16 [8, 2048, 2048], P('sp', 'tp'), may hold values from -0.125 to 0.125
- gain_moe: float32 [2048], replicated, may hold values from 0.1 to 1.9
Outputs:
- layer_out: bfloat16 [1024, 2048], P(('sp', 'tp'))
Inputs may be any that keep to these rules, and one draw needn't show every extreme that they name: `routes`: each row names 4 different experts. In each aligned block of 32 rows (the rows of one device) no expert is named by more than 32 rows, a bound that some block reaches.
All inputs are finite; a program needn't handle non-finite values.
Results may differ from a plain program's by a relative error of at most 0.017.
The roundings to bfloat16 on the way count: a program that leaves them out, or rounds other values in their place, can miss the bound.
Values may be sent and summed in bfloat16 or wider, within the bound.
No kernel may reach another device: no remote copies, remote signals or barrier semaphores. Data moves between devices by JAX's collectives and lax.ppermute only.
A program may use at most 128 MiB of HBM per device.

v0:
```python
import math
import jax
import jax.numpy as jnp
from jax import lax
from jax.sharding import PartitionSpec as P

TOP = 4
GRID_W = 64
norm_eps = 1e-06
rope_theta = 10000.0
clamp_limit = 7.0
swish_alpha = 1.702


def rope_tables(positions, head_size):
    row_index = (positions // GRID_W).astype(jnp.float32)
    col_index = (positions % GRID_W).astype(jnp.float32)
    freq_count = head_size // 4
    inverse = rope_theta ** (-jnp.arange(freq_count, dtype=jnp.float32) / freq_count)
    angles = jnp.stack([row_index[:, None] * inverse, col_index[:, None] * inverse], axis=1)
    return (jnp.cos(angles), jnp.sin(angles))


def turn(array_in, cosine_table, sine_table):
    token_count, head_count, head_size = array_in.shape
    split_field = array_in.reshape(token_count, head_count, 2, 2, head_size // 4)
    first_half = split_field[:, :, :, 0, :]
    second_half = split_field[:, :, :, 1, :]
    cos_wide = cosine_table[:, None]
    sin_wide = sine_table[:, None]
    turned = jnp.stack(
        [
            first_half * cos_wide - second_half * sin_wide,
            second_half * cos_wide + first_half * sin_wide,
        ],
        axis=3,
    )
    return turned.reshape(token_count, head_count, head_size)


def scale_rows(array_in, gain_vec):
    return (
        array_in
        * lax.rsqrt(jnp.mean(array_in * array_in, axis=-1, keepdims=True) + norm_eps)
        * gain_vec
    )


def slot_table(route_rows, experts, capacity):
    flat_routes = route_rows.reshape(-1)
    expert_hits = (flat_routes[:, None] == jnp.arange(experts, dtype=jnp.int32)[None, :]).astype(
        jnp.int32
    )
    slot_index = jnp.sum((jnp.cumsum(expert_hits, axis=0) - expert_hits) * expert_hits, axis=1)
    target = flat_routes * capacity + slot_index
    slot_onehot = target[:, None] == jnp.arange(experts * capacity, dtype=jnp.int32)[None, :]
    return slot_onehot.astype(jnp.bfloat16).reshape(
        route_rows.shape[0], route_rows.shape[1], experts * capacity
    )


def expert_apply(arrived_rows, w_gate, w_up, w_down):
    gate_pre = jnp.minimum(
        jnp.einsum("serd,edf->serf", arrived_rows, w_gate, preferred_element_type=jnp.float32),
        clamp_limit,
    )
    up_pre = jnp.clip(
        jnp.einsum("serd,edf->serf", arrived_rows, w_up, preferred_element_type=jnp.float32),
        -clamp_limit,
        clamp_limit,
    )
    active = (gate_pre * jax.nn.sigmoid(swish_alpha * gate_pre) * (up_pre + 1.0)).astype(
        jnp.bfloat16
    )
    partial_value = jnp.einsum("serf,efd->serd", active, w_down, preferred_element_type=jnp.float32)
    return lax.optimization_barrier(partial_value.astype(jnp.bfloat16)).astype(jnp.float32)


def send_back(finished):
    return lax.all_to_all(finished, "sp", split_axis=0, concat_axis=0, tiled=True)


def on_device(
    queries,
    keys,
    values,
    q_gain,
    k_gain,
    w_out,
    residual,
    gain_mix,
    gain_pre,
    routes,
    route_weights,
    w_gate,
    w_up,
    w_down,
    gain_moe,
):
    tok_rows, head_local, head_size = queries.shape
    kv_local = keys.shape[1]
    group_size = head_local // kv_local
    positions = lax.axis_index("sp") * tok_rows + jnp.arange(tok_rows, dtype=jnp.int32)
    cosine_table, sine_table = rope_tables(positions, head_size)
    q_turned = (
        turn(scale_rows(queries.astype(jnp.float32), q_gain), cosine_table, sine_table)
        * head_size ** (-0.5)
    ).astype(jnp.bfloat16)
    k_turned = turn(scale_rows(keys.astype(jnp.float32), k_gain), cosine_table, sine_table).astype(
        jnp.bfloat16
    )
    q_grouped = q_turned.reshape(tok_rows, kv_local, group_size, head_size)
    initial = (
        jnp.full((kv_local, group_size, tok_rows), -jnp.inf, jnp.float32),
        jnp.zeros((kv_local, group_size, tok_rows), jnp.float32),
        jnp.zeros((kv_local, group_size, tok_rows, head_size), jnp.float32),
    )
    carry_state = initial
    key_piece = lax.all_gather(k_turned, "sp", axis=0, tiled=True)
    value_piece = lax.all_gather(values, "sp", axis=0, tiled=True)
    piece_rows = key_piece.shape[0]
    block_rows = math.gcd(piece_rows, 1024)
    key_blocks = key_piece.reshape(piece_rows // block_rows, block_rows, kv_local, head_size)
    value_blocks = value_piece.reshape(piece_rows // block_rows, block_rows, kv_local, head_size)

    def absorb_block(state_now, key_value):
        running_max, running_sum, weighted = state_now
        key_block, value_block = key_value
        scores = jnp.einsum(
            "qkgd,skd->kgqs", q_grouped, key_block, preferred_element_type=jnp.float32
        )
        new_max = jnp.maximum(running_max, jnp.max(scores, axis=-1))
        rescale = jnp.exp(running_max - new_max)
        unnorm = jnp.exp(scores - new_max[..., None])
        running_sum = running_sum * rescale + jnp.sum(unnorm, axis=-1)
        weighted = weighted * rescale[..., None] + jnp.einsum(
            "kgqs,skd->kgqd",
            unnorm.astype(jnp.bfloat16),
            value_block,
            preferred_element_type=jnp.float32,
        )
        return ((new_max, running_sum, weighted), None)

    carry_state, ignored = lax.scan(absorb_block, carry_state, (key_blocks, value_blocks))
    running_max, running_sum, weighted = carry_state
    mixed_heads = (weighted / running_sum[..., None]).transpose(2, 0, 1, 3)
    mixed_heads = mixed_heads.reshape(tok_rows, head_local * head_size).astype(jnp.bfloat16)
    tok_part = residual.shape[0]
    width = residual.shape[1]
    projected = lax.psum_scatter(
        jnp.dot(mixed_heads, w_out, preferred_element_type=jnp.float32).astype(jnp.bfloat16),
        "tp",
        scatter_dimension=0,
        tiled=True,
    ).astype(jnp.float32)
    middle = residual.astype(jnp.float32) + scale_rows(projected, gain_mix)
    normed = scale_rows(middle, gain_pre).astype(jnp.bfloat16)
    local_experts = w_gate.shape[0]
    experts_all = local_experts * lax.axis_size("sp")
    capacity = max(2, (2 * tok_part * TOP + experts_all - 1) // experts_all)
    tables = slot_table(routes, experts_all, capacity)
    chosen = jnp.sum(tables, axis=1)
    outbound = jnp.einsum("tp,td->pd", chosen, normed, preferred_element_type=jnp.float32)
    outbound = outbound.astype(jnp.bfloat16).reshape(experts_all, capacity, width)
    arrived_rows = lax.all_gather(
        lax.all_to_all(outbound, "sp", split_axis=0, concat_axis=0, tiled=True),
        "tp",
        axis=0,
        tiled=True,
    )
    leading = arrived_rows.shape[0] // local_experts
    partial_value = expert_apply(
        arrived_rows.reshape(leading, local_experts, arrived_rows.shape[1], width),
        w_gate,
        w_up,
        w_down,
    )
    summed = lax.psum_scatter(
        partial_value.reshape(arrived_rows.shape).astype(jnp.bfloat16),
        "tp",
        scatter_dimension=0,
        tiled=True,
    )
    returned = send_back(summed)
    gathered = jnp.einsum(
        "tkp,pd->tkd",
        tables,
        returned.reshape(experts_all * capacity, width),
        preferred_element_type=jnp.float32,
    )
    mixture = jnp.sum(gathered * route_weights[:, :, None], axis=1)
    return (middle + scale_rows(mixture, gain_moe)).astype(jnp.bfloat16)


def solution(mesh):
    placed = (
        P("sp", "tp", None),
        P("sp", "tp", None),
        P("sp", "tp", None),
        P(),
        P(),
        P("tp", None),
        P(("sp", "tp"), None),
        P(),
        P(),
        P(("sp", "tp"), None),
        P(("sp", "tp"), None),
        P("sp", None, "tp"),
        P("sp", None, "tp"),
        P("sp", "tp", None),
        P(),
    )
    return jax.shard_map(
        on_device, mesh=mesh, in_specs=placed, out_specs=P(("sp", "tp"), None), check_vma=False
    )
```

profile of v0, /device:TPU:0, one launch (start us, length us, event | category | flops | bytes accessed | tf_op | source)
XLA Modules:
  0.0 267.1 jit_solution(2984971475194426291)
XLA Ops:
  6.6 1.1 copy.57
  7.8 0.1 fusion.58
  7.9 0.7 fusion.46
  8.7 0.1 copy.58
  8.9 1.0 copy.61
  9.8 1.2 copy.59
  11.1 0.8 fusion.37
  11.9 29.6 %all_gather.10 = bf16[1024,2,128]{0,2,1:T(8,128)(2,1)S(1)} all-gather(bf16[128,2,128]{0,2,1:T(8,128)(2,1)S(1)} %copy.61), channel_id=1, replica_groups=mesh['sp'=8,'tp'=4] {'sp'}, dimensions={0}, use_global_device_ids=true | all-gather | bytes 589824 | tf_op jit(solution)/shard_map/all_gather | solution.py:120
  41.5 31.4 %all_gather.9 = bf16[1024,2,128]{2,0,1:T(8,128)(2,1)S(1)} all-gather(bf16[128,2,128]{2,0,1:T(8,128)(2,1)S(1)} %copy.58), channel_id=1, replica_groups=mesh['sp'=8,'tp'=4] {'sp'}, dimensions={0}, use_global_device_ids=true | all-gather | bytes 589824 | tf_op jit(solution)/shard_map/all_gather | solution.py:119
  73.0 0.7 bitcast_reduce_fusion
  73.7 0.6 fusion.1
  74.3 0.9 fusion.31
  75.2 1.3 copy-done.1
  76.5 1.5 convolution_convert_fusion.1
  78.2 0.1 eq.53
  78.5 0.2 reduce_window_sum.11
  78.6 0.2 select_reduce_fusion
  78.8 0.1 reduce_sum.95
  79.0 0.1 fusion.54
  79.1 20.0 %reduce-scatter.3.cloned.1.call-done = bf16[32,2048]{1,0:T(8,128)(2,1)} async-done(((bf16[128,2048]{1,0:T(8,128)(2,1)}), bf16[32,2048]{1,0:T(8,128)(2,1)}) %reduce-scatter.3.cloned.1.call-update) | async-done | bytes 131088 | tf_op jit(solution)/shard_map/reduce_scatter | solution.py:150
  99.1 1.0 fusion.42
  100.2 1.1 multiply_reduce_fusion.1
  101.4 1.4 convolution_convert_fusion
  102.8 31.0 %all_to_all.10 = bf16[8,32,2048]{2,1,0:T(8,128)(2,1)} all-to-all(bf16[8,32,2048]{2,1,0:T(8,128)(2,1)S(1)} %bitcast.129), channel_id=1, replica_groups=mesh['sp'=8,'tp'=4] {'sp'}, dimensions={0} | all-to-all | bytes 2097152 | tf_op jit(solution)/shard_map/all_to_all | solution.py:166
  133.8 32.6 %all-gather.2.cloned.1.call-done = bf16[32,32,2048]{2,1,0:T(8,128)(2,1)} async-done(((bf16[8,32,2048]{2,1,0:T(8,128)(2,1)}), bf16[32,32,2048]{2,1,0:T(8,128)(2,1)}) %all-gather.2.cloned.1.call-update) | async-done | bytes 4194320 | tf_op jit(solution)/shard_map/all_gather | solution.py:165
  166.5 6.6 %fusion.7 = f32[32,32,512]{2,1,0:T(8,128)} fusion(bf16[32,32,2048]{2,1,0:T(8,128)(2,1)} %all-gather.2.cloned.1.call-done, bf16[1,2048,512]{2,1,0:T(8,128)(2,1)} %param.27), kind=kOutput, calls=%fused_computation.13 | convolution fusion | flops 2147483648 | bytes 8388608 | tf_op jit(solution)/shard_map/serd,edf->serf/dot_general | solution.py:68
  173.1 10.3 %convert_bitcast_fusion = bf16[32,1,32,2048]{3,2,0,1:T(8,128)(2,1)} fusion(bf16[1,512,2048]{2,1,0:T(8,128)(2,1)S(1)} %copy-done, f32[32,32,512]{2,1,0:T(8,128)} %fusion.7, bf16[32,32,2048]{2,1,0:T(8,128)(2,1)} %all-gather.2.cloned.1.call-done, bf16[1,2048,512]{2,1,0:T(8,128)(2,1)} %param.26), kind=kOutput, calls=%fused_computation.3 | convolution fusion | flops 4302307328 | bytes 14680064 | tf_op jit(solution)/shard_map/serf,efd->serd/dot_general | solution.py:75
  183.4 44.7 %reduce-scatter.5.cloned.1.call-done = bf16[8,32,2048]{2,1,0:T(8,128)(2,1)} async-done(((bf16[32,32,2048]{2,1,0:T(8,128)(2,1)}), bf16[8,32,2048]{2,1,0:T(8,128)(2,1)}) %reduce-scatter.5.cloned.1.call-update) | async-done | bytes 1048592 | tf_op jit(solution)/shard_map/reduce_scatter | solution.py:178
  228.1 31.1 %all_to_all.11 = bf16[8,32,2048]{2,1,0:T(8,128)(2,1)S(1)} all-to-all(bf16[8,32,2048]{2,1,0:T(8,128)(2,1)} %reduce-scatter.5.cloned.1.call-done), channel_id=1, replica_groups=mesh['sp'=8,'tp'=4] {'sp'}, dimensions={0} | all-to-all | bytes 2097152 | tf_op jit(solution)/shard_map/all_to_all | solution.py:80
  259.2 0.3 fusion.21
  259.6 0.1 multiply_reduce_fusion
  259.8 0.8 add_convert_fusion
  (43 shorter events, 0.9 us)
Async XLA Ops:
  6.5 166.5 %copy-start = (bf16[1,512,2048]{2,1,0:T(8,128)(2,1)S(1)}, bf16[1,512,2048]{2,1,0:T(8,128)(2,1)}, u32[]{:S(2)}) copy-start(bf16[1,512,2048]{2,1,0:T(8,128)(2,1)} %param.28) | copy-start | bytes 6291460
  6.5 92.6 %reduce-scatter.3.cloned.1.call-start = ((), (), s32[]{:S(2)}) async-start(), calls=%async_computation.4 | async-start | bytes 655360 | tf_op jit(solution)/shard_map/reduce_scatter | solution.py:150
  74.3 2.2 copy-start.1
  76.5 1.6 copy-start.7
  76.5 23.6 %copy-start.3 = (bf16[32,2048]{1,0:T(8,128)(2,1)S(1)}, bf16[32,2048]{1,0:T(8,128)(2,1)}, u32[]{:S(2)}) copy-start(bf16[32,2048]{1,0:T(8,128)(2,1)} %param.21) | copy-start | bytes 393220
  76.5 23.7 %copy-start.4 = (f32[2048]{0:T(1024)S(1)}, f32[2048]{0:T(1024)}, u32[]{:S(2)}) copy-start(f32[2048]{0:T(1024)} %param.22) | copy-start | bytes 24580
  76.5 24.8 %copy-start.5 = (f32[2048]{0:T(1024)S(1)}, f32[2048]{0:T(1024)}, u32[]{:S(2)}) copy-start(f32[2048]{0:T(1024)} %param.23) | copy-start | bytes 24580
  78.1 88.4 %all-gather.2.cloned.1.call-start = ((), (), s32[]{:S(2)}) async-start(), calls=%async_computation.5 | async-start | bytes 5242880 | tf_op jit(solution)/shard_map/all_gather | solution.py:165
  133.8 94.3 %reduce-scatter.5.cloned.1.call-start = ((), (), s32[]{:S(2)}) async-start(), calls=%async_computation.6 | async-start | bytes 5242880 | tf_op jit(solution)/shard_map/reduce_scatter | solution.py:178
  183.4 75.8 %copy-start.8 = (f32[32,4]{0,1:T(4,128)S(1)}, f32[32,4]{0,1:T(4,128)}, u32[]{:S(2)}) copy-start(f32[32,4]{0,1:T(4,128)} %param.25) | copy-start | bytes 1540
  183.4 76.3 %copy-start.2 = (bf16[32,2048]{1,0:T(8,128)(2,1)S(1)}, bf16[32,2048]{1,0:T(8,128)(2,1)}, u32[]{:S(2)}) copy-start(bf16[32,2048]{1,0:T(8,128)(2,1)} %reduce-scatter.3.cloned.1.call-done) | copy-start | bytes 393220
  183.4 76.3 %copy-start.6 = (f32[2048]{0:T(1024)S(1)}, f32[2048]{0:T(1024)}, u32[]{:S(2)}) copy-start(f32[2048]{0:T(1024)} %param.29) | copy-start | bytes 24580
Sparse Core Ops, SparseCore 0:
  78.2 20.8 reduce-scatter.2
  133.9 32.5 all-gather.1
  183.5 44.5 reduce-scatter.4
where the time goes:
time: 268 us; the launch traced here: 267 us
  blocking collectives  123 us (46%)
  waiting for transfers between devices  97.4 us (36%)
  matrix products  21.8 us (8%)
  between operations  13.4 us (5%)
  other arithmetic  6.28 us (2%)
  local copies, waits for them, and re-layouts  5.04 us (2%)
    reduce_scatter x1, waiting for transfers between devices, on_device(): lax.psum_scatter(partial_value.reshape(arrived_rows.shape).astype(jnp.bfl...  44.7 us
    all_gather x1, waiting for transfers between devices, on_device(): lax.all_gather(lax.all_to_all(outbound, 'sp', split_axis=0, concat_axis=0...  32.6 us
    all_gather x1, blocking collectives, on_device(): key_piece = lax.all_gather(k_turned, 'sp', axis=0, tiled=True)  31.4 us
    all_to_all x1, blocking collectives, send_back(): lax.all_to_all(finished, 'sp', split_axis=0, concat_axis=0, tiled=True)  31.1 us
    all_to_all x1, blocking collectives, on_device(): lax.all_to_all(outbound, 'sp', split_axis=0, concat_axis=0, tiled=True)  31 us
    all_gather x1, blocking collectives, on_device(): value_piece = lax.all_gather(values, 'sp', axis=0, tiled=True)  29.6 us
    reduce_scatter x1, waiting for transfers between devices, on_device(): lax.psum_scatter(jnp.dot(mixed_heads, w_out, preferred_element_type=jnp.f...  20 us
    dot_general x1, matrix products, expert_apply(): jnp.einsum('serf,efd->serd', active, w_down, preferred_element_type=jnp.f...  10.3 us
  transfers between devices with their start and end apart: 3, of which 3 were waited for; matrix products, arithmetic and copies ran while one was open for 0% of the time, Pallas kernels for 0%

commit v1 on v0

--- a/solution.py
+++ b/solution.py
@@ -116,8 +116,11 @@
         jnp.zeros((kv_local, group_size, tok_rows, head_size), jnp.float32),
     )
     carry_state = initial
-    key_piece = lax.all_gather(k_turned, "sp", axis=0, tiled=True)
-    value_piece = lax.all_gather(values, "sp", axis=0, tiled=True)
+    key_piece, value_piece = jnp.split(
+        lax.all_gather(jnp.concatenate([k_turned, values], axis=1), "sp", axis=0, tiled=True),
+        [k_turned.shape[1]],
+        axis=1,
+    )
     piece_rows = key_piece.shape[0]
     block_rows = math.gcd(piece_rows, 1024)
     key_blocks = key_piece.reshape(piece_rows // block_rows, block_rows, kv_local, head_size)

time: 268 us -> 249 us (0.929)
  blocking collectives: 123 us -> 62.1 us
  waiting for transfers between devices: 97.4 us -> 139 us
    all_gather x2 -> x0, blocking collectives: 61 us -> none  [the longest x1 31.4 us: on_device(): key_piece = lax.all_gather(k_turned, 'sp', axis=0, tiled=True)]
    all_gather x0 -> x1, waiting for transfers between devices: none -> 41.6 us  [on_device(): lax.all_gather(jnp.concatenate([k_turned, values], axis=1), 'sp', axis=0,...]
  transfers between devices with their start and end apart: 3 -> 4, of which waited for: 3 -> 4; matrix products, arithmetic and copies ran while one was open for 0% -> 1% of each run, Pallas kernels for 0% -> 0%
where the time goes in v1:
time: 249 us
  waiting for transfers between devices  139 us (56%)
  blocking collectives  62.1 us (25%)
  matrix products  22.7 us (9%)
  between operations  13.4 us (5%)
  other arithmetic  6.28 us (3%)
  local copies, waits for them, and re-layouts  5.7 us (2%)
    reduce_scatter x1, waiting for transfers between devices, on_device(): lax.psum_scatter(partial_value.reshape(arrived_rows.shape).astype(jnp.bfl...  44.7 us
    all_gather x1, waiting for transfers between devices, on_device(): lax.all_gather(jnp.concatenate([k_turned, values], axis=1), 'sp', axis=0,...  41.6 us
    all_gather x1, waiting for transfers between devices, on_device(): lax.all_gather(lax.all_to_all(outbound, 'sp', split_axis=0, concat_axis=0...  32.6 us
    all_to_all x1, blocking collectives, send_back(): lax.all_to_all(finished, 'sp', split_axis=0, concat_axis=0, tiled=True)  31.1 us
    all_to_all x1, blocking collectives, on_device(): lax.all_to_all(outbound, 'sp', split_axis=0, concat_axis=0, tiled=True)  31 us
    reduce_scatter x1, waiting for transfers between devices, on_device(): lax.psum_scatter(jnp.dot(mixed_heads, w_out, preferred_element_type=jnp.f...  19.5 us
    dot_general x1, matrix products, expert_apply(): jnp.einsum('serf,efd->serd', active, w_down, preferred_element_type=jnp.f...  10.3 us
    dot_general x1, matrix products, expert_apply(): jnp.einsum('serd,edf->serf', arrived_rows, w_up, preferred_element_type=j...  6.59 us
  transfers between devices with their start and end apart: 4, of which 4 were waited for; matrix products, arithmetic and copies ran while one was open for 1% of the time, Pallas kernels for 0%

profile of v1, /device:TPU:0, one launch (start us, length us, event | category | flops | bytes accessed | tf_op | source)
XLA Modules:
  0.0 248.9 jit_solution(15564540216927653685)
XLA Ops:
  6.6 1.1 copy.61
  7.8 0.1 fusion.56
  7.9 0.7 fusion.44
  8.7 0.1 copy.62
  8.9 0.9 copy.63
  9.7 0.7 pad_maximum_fusion
  10.5 1.2 copy.64
  11.7 0.1 fusion.37
  12.0 41.6 %all-gather.3.cloned.1.call-done = bf16[1024,4,128]{2,0,1:T(8,128)(2,1)} async-done(((bf16[128,4,128]{2,0,1:T(8,128)(2,1)}), bf16[1024,4,128]{2,0,1:T(8,128)(2,1)}) %all-gather.3.cloned.1.call-update) | async-done | bytes 1048592 | tf_op jit(solution)/shard_map/all_gather | solution.py:120
  53.6 1.7 bitcast_reduce_fusion
  55.3 0.6 fusion.1
  55.9 0.6 copy-done.4
  56.5 0.8 fusion.31
  57.3 1.4 copy-done.1
  58.7 1.5 convolution_convert_fusion.1
  60.5 0.1 eq.53
  60.7 0.2 reduce_window_sum.11
  60.8 0.2 select_reduce_fusion
  61.0 0.1 reduce_sum.95
  61.3 19.5 %reduce-scatter.3.cloned.1.call-done = bf16[32,2048]{1,0:T(8,128)(2,1)} async-done(((bf16[128,2048]{1,0:T(8,128)(2,1)}), bf16[32,2048]{1,0:T(8,128)(2,1)}) %reduce-scatter.3.cloned.1.call-update) | async-done | bytes 131088 | tf_op jit(solution)/shard_map/reduce_scatter | solution.py:153
  80.9 1.0 fusion.40
  81.9 1.1 multiply_reduce_fusion.1
  83.1 1.4 convolution_convert_fusion
  84.5 31.0 %all_to_all.10 = bf16[8,32,2048]{2,1,0:T(8,128)(2,1)} all-to-all(bf16[8,32,2048]{2,1,0:T(8,128)(2,1)S(1)} %bitcast.129), channel_id=1, replica_groups=mesh['sp'=8,'tp'=4] {'sp'}, dimensions={0} | all-to-all | bytes 2097152 | tf_op jit(solution)/shard_map/all_to_all | solution.py:169
  115.6 32.6 %all-gather.5.cloned.1.call-done = bf16[32,32,2048]{2,1,0:T(8,128)(2,1)} async-done(((bf16[8,32,2048]{2,1,0:T(8,128)(2,1)}), bf16[32,32,2048]{2,1,0:T(8,128)(2,1)}) %all-gather.5.cloned.1.call-update) | async-done | bytes 4194320 | tf_op jit(solution)/shard_map/all_gather | solution.py:168
  148.2 6.6 %fusion.7 = f32[32,32,512]{2,1,0:T(8,128)} fusion(bf16[32,32,2048]{2,1,0:T(8,128)(2,1)} %all-gather.5.cloned.1.call-done, bf16[1,2048,512]{2,1,0:T(8,128)(2,1)} %param.27), kind=kOutput, calls=%fused_computation.13 | convolution fusion | flops 2147483648 | bytes 8388608 | tf_op jit(solution)/shard_map/serd,edf->serf/dot_general | solution.py:68
  154.8 10.3 %convert_bitcast_fusion = bf16[32,1,32,2048]{3,2,0,1:T(8,128)(2,1)} fusion(bf16[1,512,2048]{2,1,0:T(8,128)(2,1)S(1)} %copy-done, f32[32,32,512]{2,1,0:T(8,128)} %fusion.7, bf16[32,32,2048]{2,1,0:T(8,128)(2,1)} %all-gather.5.cloned.1.call-done, bf16[1,2048,512]{2,1,0:T(8,128)(2,1)} %param.26), kind=kOutput, calls=%fused_computation.3 | convolution fusion | flops 4302307328 | bytes 14680064 | tf_op jit(solution)/shard_map/serf,efd->serd/dot_general | solution.py:75
  165.2 44.7 %reduce-scatter.5.cloned.1.call-done = bf16[8,32,2048]{2,1,0:T(8,128)(2,1)} async-done(((bf16[32,32,2048]{2,1,0:T(8,128)(2,1)}), bf16[8,32,2048]{2,1,0:T(8,128)(2,1)}) %reduce-scatter.5.cloned.1.call-update) | async-done | bytes 1048592 | tf_op jit(solution)/shard_map/reduce_scatter | solution.py:181
  209.9 31.1 %all_to_all.11 = bf16[8,32,2048]{2,1,0:T(8,128)(2,1)S(1)} all-to-all(bf16[8,32,2048]{2,1,0:T(8,128)(2,1)} %reduce-scatter.5.cloned.1.call-done), channel_id=1, replica_groups=mesh['sp'=8,'tp'=4] {'sp'}, dimensions={0} | all-to-all | bytes 2097152 | tf_op jit(solution)/shard_map/all_to_all | solution.py:80
  241.0 0.3 fusion.21
  241.4 0.1 multiply_reduce_fusion
  241.5 0.8 add_convert_fusion
  (49 shorter events, 1.0 us)
Async XLA Ops:
  6.5 148.3 %copy-start = (bf16[1,512,2048]{2,1,0:T(8,128)(2,1)S(1)}, bf16[1,512,2048]{2,1,0:T(8,128)(2,1)}, u32[]{:S(2)}) copy-start(bf16[1,512,2048]{2,1,0:T(8,128)(2,1)} %param.28) | copy-start | bytes 6291460
  6.5 5.2 %copy-start.10 = (f32[128]{0:T(128)S(1)}, f32[128]{0:T(128)}, u32[]{:S(2)}) copy-start(f32[128]{0:T(128)} %param.18) | copy-start | bytes 1540
  6.5 47.0 %all-gather.3.cloned.1.call-start = ((), (), s32[]{:S(2)}) async-start(), calls=%async_computation.4 | async-start | bytes 1179648 | tf_op jit(solution)/shard_map/all_gather | solution.py:120
  10.4 70.4 %reduce-scatter.3.cloned.1.call-start = ((), (), s32[]{:S(2)}) async-start(), calls=%async_computation.5 | async-start | bytes 655360 | tf_op jit(solution)/shard_map/reduce_scatter | solution.py:153
  55.3 1.2 copy-start.4
  56.5 2.2 copy-start.1
  58.7 1.6 copy-start.8
  58.7 23.2 %copy-start.3 = (bf16[32,2048]{1,0:T(8,128)(2,1)S(1)}, bf16[32,2048]{1,0:T(8,128)(2,1)}, u32[]{:S(2)}) copy-start(bf16[32,2048]{1,0:T(8,128)(2,1)} %param.21) | copy-start | bytes 393220
  58.7 23.2 %copy-start.5 = (f32[2048]{0:T(1024)S(1)}, f32[2048]{0:T(1024)}, u32[]{:S(2)}) copy-start(f32[2048]{0:T(1024)} %param.22) | copy-start | bytes 24580
  58.7 24.3 %copy-start.6 = (f32[2048]{0:T(1024)S(1)}, f32[2048]{0:T(1024)}, u32[]{:S(2)}) copy-start(f32[2048]{0:T(1024)} %param.23) | copy-start | bytes 24580
  60.3 87.9 %all-gather.5.cloned.1.call-start = ((), (), s32[]{:S(2)}) async-start(), calls=%async_computation.6 | async-start | bytes 5242880 | tf_op jit(solution)/shard_map/all_gather | solution.py:168
  115.5 94.3 %reduce-scatter.5.cloned.1.call-start = ((), (), s32[]{:S(2)}) async-start(), calls=%async_computation.7 | async-start | bytes 5242880 | tf_op jit(solution)/shard_map/reduce_scatter | solution.py:181
  165.2 75.8 %copy-start.9 = (f32[32,4]{0,1:T(4,128)S(1)}, f32[32,4]{0,1:T(4,128)}, u32[]{:S(2)}) copy-start(f32[32,4]{0,1:T(4,128)} %param.25) | copy-start | bytes 1540
  165.2 76.3 %copy-start.2 = (bf16[32,2048]{1,0:T(8,128)(2,1)S(1)}, bf16[32,2048]{1,0:T(8,128)(2,1)}, u32[]{:S(2)}) copy-start(bf16[32,2048]{1,0:T(8,128)(2,1)} %reduce-scatter.3.cloned.1.call-done) | copy-start | bytes 393220
  165.2 76.3 %copy-start.7 = (f32[2048]{0:T(1024)S(1)}, f32[2048]{0:T(1024)}, u32[]{:S(2)}) copy-start(f32[2048]{0:T(1024)} %param.29) | copy-start | bytes 24580
Sparse Core Ops, SparseCore 0:
  10.5 42.9 all-gather.2
  60.4 20.3 reduce-scatter.2
  115.7 32.5 all-gather.4
  165.3 44.5 reduce-scatter.4
